TPU v7x, 32 devices: a whole 2x2x4 slice. The times are simulated.
32 devices in a mesh: fs: 8 (over z, y), tp: 4 (over x, core).
Axes of the slice: x: 2, y: 2, z: 4, core: 2. Of those that a mesh axis runs over, the one named last changes fastest.
Arguments:
- prompt: bfloat16 [4096, 2048], P(('fs', 'tp')), may hold values from -6 to 6
- norm_gain: float32 [2048], P('fs'), may hold values from 0.1 to 1.9
- up_trained: float32 [2048, 8192], P('fs', 'tp'), may hold values from -0.125 to 0.125
- down_trained: float32 [2048, 8192], P('fs', 'tp'), may hold values from -0.0625 to 0.0625
Outputs:
- up_served: bfloat16 [2048, 8192], P(None, 'tp')
- down_served: bfloat16 [8192, 2048], P('tp')
- mixed: bfloat16 [4096, 2048], P(('fs', 'tp'))
All inputs are finite; a program needn't handle non-finite values.
Results may differ from a plain program's by a relative error of at most 0.014.
Values may be sent and summed in bfloat16 or wider, within the bound.
A program may use at most 128 MiB of HBM per device.

v0:
```python
import functools

import jax
import jax.numpy as jnp
from jax import lax
from jax.experimental import pallas as pl
from jax.experimental.pallas import tpu as pltpu
from jax.sharding import PartitionSpec as P

MESH = pl.DeviceIdType.MESH
PIECES = 2
LIMIT = 40


def factor(fs):
    ny = 1
    while ny * 2 * ny * 2 <= fs:
        ny *= 2
    return fs // ny, ny


def turns(rows):
    return rows % 128 == 0


def flush(up_in, down_in, mixed_in, up_out, down_out, mixed_out, sems):
    copies = [
        pltpu.make_async_copy(source, target, sems.at[i])
        for i, (source, target) in enumerate(((up_in, up_out), (down_in, down_out), (mixed_in, mixed_out)))
    ]
    for copy in copies:
        copy.start()
    for copy in copies:
        copy.wait()


def kernel(nz, ny, tp, prompt, gain, up_f, down_f, up_all, down_out, mixed,
           down_scratch, norm_all, hidden, part_send, part_recv,
           w_send, w_recv, n_send, n_recv, p_send, p_recv):
    fs = nz * ny
    rows, width = up_f.shape
    tile = 256
    turned = turns(rows)
    down_all = down_scratch if turned else down_out
    piece = rows // PIECES
    tokens = prompt.shape[0]
    me = lax.axis_index("fs")
    t = lax.axis_index("tp")
    z, y = me // ny, lax.rem(me, ny)
    exists = (z < nz - 1, z > 0, y < ny - 1, y > 0)
    step = (ny, -ny, 1, -1)
    trick = ny == 2 and nz % 2 == 0
    half = PIECES // 2
    even = lax.rem(z, 2) == 0
    mate = z + 1 - 2 * lax.rem(z, 2)
    buffers = (up_all, down_all)
    sent = []

    barrier = pltpu.get_barrier_semaphore()
    for direction in range(4):
        @pl.when(exists[direction])
        def _():
            pl.semaphore_signal(barrier, inc=1, device_id={"fs": me + step[direction]}, device_id_type=MESH)
    for offset in range(1, tp):
        pl.semaphore_signal(barrier, inc=1, device_id={"tp": lax.rem(t + offset, tp)}, device_id_type=MESH)

    def weights(phase, block, c, direction):
        start = pl.multiple_of(block * rows + c * piece, piece)
        ref = buffers[phase].at[pl.ds(start, piece)]
        slot = (phase * fs + block) * PIECES + c
        return pltpu.make_async_remote_copy(
            src_ref=ref, dst_ref=ref,
            send_sem=w_send.at[direction, slot], recv_sem=w_recv.at[slot],
            device_id={"fs": me + step[direction]}, device_id_type=MESH)

    def send(condition, phase, block, c, direction):
        condition = jnp.logical_and(condition, exists[direction])
        sent.append((condition, phase, block, c, direction))

        @pl.when(condition)
        def _():
            weights(phase, block, c, direction).start()

    def arrive(condition, phase, block, c):
        @pl.when(condition)
        def _():
            weights(phase, block, c, 0).wait_recv()

    for c in range(PIECES):
        where = pl.ds(pl.multiple_of(me * rows + c * piece, piece), piece)
        part = slice(c * piece, (c + 1) * piece)
        up_all[where, :] = (gain[part, :] * up_f[part, :]).astype(jnp.bfloat16)
    pl.semaphore_wait(barrier, sum(e.astype(jnp.int32) for e in exists) + tp - 1)
    always = z >= 0
    for c in range(PIECES):
        for direction in range(4):
            send(always, 0, me, c, direction)

    values = prompt[...].astype(jnp.float32)
    scale = lax.rsqrt(jnp.mean(values * values, axis=-1, keepdims=True) + 1e-06)
    mine = pl.ds(pl.multiple_of(t * tokens, tokens), tokens)
    norm_all[mine, :] = (values * scale).astype(jnp.bfloat16)
    for c in range(PIECES):
        where = pl.ds(pl.multiple_of(me * rows + c * piece, piece), piece)
        part = slice(c * piece, (c + 1) * piece)
        down_all[where, :] = down_f[part, :].astype(jnp.bfloat16)

    def token_copy(offset):
        return pltpu.make_async_remote_copy(
            src_ref=norm_all.at[mine], dst_ref=norm_all.at[mine],
            send_sem=n_send.at[offset], recv_sem=n_recv.at[t],
            device_id={"tp": lax.rem(t + offset, tp)}, device_id_type=MESH)

    def token_arrival(offset):
        source = lax.rem(t + offset, tp)
        ref = norm_all.at[pl.ds(pl.multiple_of(source * tokens, tokens), tokens)]
        return pltpu.make_async_remote_copy(
            src_ref=ref, dst_ref=ref, send_sem=n_send.at[offset], recv_sem=n_recv.at[source],
            device_id={"tp": source}, device_id_type=MESH)

    for offset in range(1, tp):
        token_copy(offset).start()
    for c in range(half):
        for direction in (2, 3):
            send(always, 1, me, c, direction)

    def own_down(d):
        for c in range(PIECES):
            send(z == d, 1, me, c, 0)
            send(z == nz - 1 - d, 1, me, c, 1)

    def column(phase, d):
        for c in range(PIECES):
            for s in (1, -1):
                zb = z + s * d
                there = jnp.logical_and(zb >= 0, zb < nz)
                block = zb * ny + y
                arrive(there, phase, block, c)
                send(there, phase, block, c, 1 if s > 0 else 0)
                across = there
                if trick and c >= half:
                    across = jnp.logical_and(there, zb != mate)
                send(across, phase, block, c, 2)
                send(across, phase, block, c, 3)

    def swap(phase):
        if not trick:
            return
        block = z * ny + 1 - y
        for c in range(half, PIECES):
            if phase == 0:
                arrive(always, phase, block, c)
            send(even, phase, block, c, 0)
            send(jnp.logical_not(even), phase, block, c, 1)

    def sideways(phase, d, s):
        zb = z + s * d
        inside = jnp.logical_and(zb >= 0, zb < nz)
        for e in range(1, ny):
            for u in (1, -1):
                yb = y + u * e
                there = jnp.logical_and(inside, jnp.logical_and(yb >= 0, yb < ny))
                for c in range(PIECES):
                    if trick and phase == 0 and d == 0 and c >= half:
                        continue
                    wanted = there
                    if trick and c >= half:
                        wanted = jnp.logical_and(there, zb != mate)
                    arrive(wanted, phase, zb * ny + yb, c)
                    if e < ny - 1:
                        send(wanted, phase, zb * ny + yb, c, 3 if u > 0 else 2)

    def swapped(phase):
        if trick:
            for c in range(half, PIECES):
                arrive(always, phase, mate * ny + 1 - y, c)

    def partial_copy(block, offset):
        peer = lax.rem(t + offset, tp)
        return pltpu.make_async_remote_copy(
            src_ref=part_send.at[block, pl.ds(pl.multiple_of(peer * tokens, tokens), tokens)],
            dst_ref=part_recv.at[t, block],
            send_sem=p_send.at[offset], recv_sem=p_recv.at[t],
            device_id={"tp": peer}, device_id_type=MESH)

    def consume(condition, block):
        @pl.when(condition)
        def _():
            where = pl.ds(pl.multiple_of(block * rows, rows), rows)
            part_send[block] = lax.dot_general(
                hidden[...], down_all[where, :], (((1,), (1,)), ((), ())),
                preferred_element_type=jnp.float32).astype(jnp.bfloat16)
            for offset in range(1, tp):
                partial_copy(block, offset).start()
            if turned:
                @pl.loop(0, width // tile)
                def _(j):
                    at = pl.ds(pl.multiple_of(j * tile, tile), tile)
                    down_out[at, where] = jnp.transpose(down_all[where, at])

    def consume_column(d):
        @pl.loop(0, 1 if d == 0 else 2)
        def _(i):
            zb = z + (1 - 2 * i) * d
            consume(jnp.logical_and(zb >= 0, zb < nz), zb * ny + y)

    def consume_sideways(d):
        @pl.loop(0, (1 if d == 0 else 2) * (ny - 1))
        def _(i):
            zb = z + (1 - 2 * (i // (ny - 1))) * d
            yb = lax.rem(y + 1 + lax.rem(i, ny - 1), ny)
            inside = jnp.logical_and(zb >= 0, zb < nz)
            if trick:
                inside = jnp.logical_and(inside, zb != mate)
            consume(inside, zb * ny + yb)

    def signs(d):
        return (1,) if d == 0 else (1, -1)

    own_down(0)
    for d in range(1, nz):
        column(0, d)
        if d == 1:
            swap(0)
        own_down(d)
    for c in range(half, PIECES):
        for direction in (2, 3):
            send(always, 1, me, c, direction)
    for d in range(nz):
        for s in signs(d):
            sideways(0, d, s)
    swapped(0)
    for offset in range(1, tp):
        token_arrival(offset).wait_recv()

    @pl.loop(0, width // tile)
    def _(j):
        at = pl.ds(pl.multiple_of(j * tile, tile), tile)
        pre = jnp.dot(norm_all[...], up_all[:, at], preferred_element_type=jnp.float32)
        hidden[:, at] = jnp.square(jnp.maximum(pre, 0.0)).astype(jnp.bfloat16)

    for d in range(1, nz):
        column(1, d)
        if d == nz - 1:
            swap(1)
        consume_column(d - 1)
        if d == 1:
            sideways(1, 0, 1)
            consume_sideways(0)
    if nz == 1:
        sideways(1, 0, 1)
        consume_sideways(0)
    consume_column(nz - 1)
    for d in range(1, nz):
        for s in signs(d):
            sideways(1, d, s)
        consume_sideways(d)
    if trick:
        swapped(1)
        consume(always, mate * ny + 1 - y)

    for offset in range(1, tp):
        source = lax.rem(t + offset, tp)
        whole = part_recv.at[source]
        arrival = pltpu.make_async_remote_copy(
            src_ref=whole, dst_ref=whole, send_sem=p_send.at[offset], recv_sem=p_recv.at[source],
            device_id={"tp": source}, device_id_type=MESH)
        arrival.wait_recv()
    for block in range(fs):
        total = part_send[block, mine, :].astype(jnp.float32)
        for offset in range(1, tp):
            total += part_recv[lax.rem(t + offset, tp), block].astype(jnp.float32)
        mixed[:, block * rows:(block + 1) * rows] = total.astype(jnp.bfloat16)

    for offset in range(1, tp):
        token_copy(offset).wait_send()
        whole = part_recv.at[t]
        pltpu.make_async_remote_copy(
            src_ref=whole, dst_ref=whole, send_sem=p_send.at[offset], recv_sem=p_recv.at[t],
            device_id={"tp": lax.rem(t + offset, tp)}, device_id_type=MESH).wait_send()
    for condition, phase, block, c, direction in sent:
        @pl.when(condition)
        def _():
            weights(phase, block, c, direction).wait_send()


def solution(mesh):
    fs, tp = mesh.shape["fs"], mesh.shape["tp"]
    nz, ny = factor(fs)

    def shards(prompt, norm_gain, up_trained, down_trained):
        rows, width = up_trained.shape
        tokens, depth = prompt.shape
        bf16 = jnp.bfloat16
        turned = turns(rows)
        down_shape = (width, depth) if turned else (depth, width)
        slots = 2 * fs * PIECES
        any_space = pl.BlockSpec(memory_space=pl.ANY)
        vmem = pl.BlockSpec(memory_space=pltpu.VMEM)
        up_whole, down_whole, mixed = pl.pallas_call(
            functools.partial(kernel, nz, ny, tp),
            out_shape=(
                pltpu.VMEM((depth, width), bf16),
                pltpu.VMEM(down_shape, bf16),
                pltpu.VMEM((tokens, depth), bf16),
            ),
            in_specs=[vmem] * 4,
            out_specs=[vmem] * 3,
            scratch_shapes=[
                pltpu.VMEM((depth, width) if turned else (16, 128), bf16),
                pltpu.VMEM((tp * tokens, depth), bf16),
                pltpu.VMEM((tp * tokens, width), bf16),
                pltpu.VMEM((fs, tp * tokens, rows), bf16),
                pltpu.VMEM((tp, fs, tokens, rows), bf16),
                pltpu.SemaphoreType.DMA((4, slots)),
                pltpu.SemaphoreType.DMA((slots,)),
                pltpu.SemaphoreType.DMA((tp,)),
                pltpu.SemaphoreType.DMA((tp,)),
                pltpu.SemaphoreType.DMA((tp,)),
                pltpu.SemaphoreType.DMA((tp,)),
            ],
            compiler_params=pltpu.CompilerParams(
                collective_id=0, has_side_effects=True, vmem_limit_bytes=LIMIT * 1024 * 1024
            ),
        )(prompt, norm_gain[:, None], up_trained, down_trained)
        up_whole, down_whole, mixed = pl.pallas_call(
            flush,
            out_shape=(
                jax.ShapeDtypeStruct((depth, width), bf16),
                jax.ShapeDtypeStruct(down_shape, bf16),
                jax.ShapeDtypeStruct((tokens, depth), bf16),
            ),
            in_specs=[vmem] * 3,
            out_specs=[any_space] * 3,
            scratch_shapes=[pltpu.SemaphoreType.DMA((3,))],
            compiler_params=pltpu.CompilerParams(vmem_limit_bytes=2 * 1024 * 1024),
        )(up_whole, down_whole, mixed)
        return up_whole, down_whole if turned else jnp.transpose(down_whole), mixed

    return jax.shard_map(
        shards,
        mesh=mesh,
        in_specs=(P(("fs", "tp"), None), P("fs"), P("fs", "tp"), P("fs", "tp")),
        out_specs=(P(None, "tp"), P("tp", None), P(("fs", "tp"), None)),
        check_vma=False,
    )
```

profile of v0, /device:TPU:0, one launch (start us, length us, event | category | flops | bytes accessed | tf_op | source)
XLA Modules:
  0.0 182.5 jit_solution(16813299848783990574)
XLA Ops:
  0.6 1.5 copy.7.gain
  2.1 174.2 %shard_map.67 = (bf16[2048,2048]{1,0:T(8,128)(2,1)S(1)}, bf16[2048,2048]{1,0:T(8,128)(2,1)S(1)}, bf16[128,2048]{1,0:T(8,128)(2,1)S(1)}) custom-call(bf16[128,2048]{1,0:T(8,128)(2,1)} %prompt.1, f32[256,1]{1,0:T(8,128)} %copy.7.gain, f32[256,2048]{1,0:T(8,128)} %up_f.1, f32[256,2048]{1,0:T(8,128)} %down_f.1), custom_call_target="tpu_custom_call" | custom-call | tf_op jit(solution)/shard_map/pallas_call | solution.py:300
  176.3 6.2 %shard_map.68 = (bf16[2048,2048]{1,0:T(8,128)(2,1)}, bf16[2048,2048]{1,0:T(8,128)(2,1)}, bf16[128,2048]{1,0:T(8,128)(2,1)}) custom-call(bf16[2048,2048]{1,0:T(8,128)(2,1)S(1)} %get-tuple-element.6.up_in, bf16[2048,2048]{1,0:T(8,128)(2,1)S(1)} %get-tuple-element.7.down_in, bf16[128,2048]{1,0:T(8,128)(2,1)S(1)} %get-tuple-element.8.mixed_in), custom_call_target="tpu_custom_call" | custom-call | tf_op jit(solution)/shard_map/pallas_call | solution.py:326
where the time goes:
time: 183 us
  Pallas kernels  180 us (98%)
    pallas_call x1, Pallas kernels, shards(): pl.pallas_call(functools.partial(kernel, nz, ny, tp), out_shape=(pltpu.VM...  174 us
    pallas_call x1, Pallas kernels, shards(): pl.pallas_call(flush, out_shape=(jax.ShapeDtypeStruct((depth, width), bf1...  6.19 us

commit v1 on v0

--- a/solution.py
+++ b/solution.py
@@ -10,6 +10,7 @@
 MESH = pl.DeviceIdType.MESH
 PIECES = 2
 LIMIT = 40
+LANES = 128
 
 
 def factor(fs):
@@ -34,9 +35,10 @@
         copy.wait()
 
 
-def kernel(nz, ny, tp, prompt, gain, up_f, down_f, up_all, down_out, mixed,
+def kernel(nz, ny, tp, prompt_hbm, gain_hbm, up_hbm, down_hbm, up_all, down_out, mixed,
+           prompt, gain_row, gain, up_f, down_f,
            down_scratch, norm_all, hidden, part_send, part_recv,
-           w_send, w_recv, n_send, n_recv, p_send, p_recv):
+           in_sems, w_send, w_recv, n_send, n_recv, p_send, p_recv):
     fs = nz * ny
     rows, width = up_f.shape
     tile = 256
@@ -56,6 +58,15 @@
     buffers = (up_all, down_all)
     sent = []
 
+    reads = [pltpu.make_async_copy(gain_hbm, gain_row, in_sems.at[0])]
+    for c in range(PIECES):
+        part = pl.ds(c * piece, piece)
+        reads.append(pltpu.make_async_copy(up_hbm.at[part], up_f.at[part], in_sems.at[1 + c]))
+    reads.append(pltpu.make_async_copy(prompt_hbm, prompt, in_sems.at[1 + PIECES]))
+    reads.append(pltpu.make_async_copy(down_hbm, down_f, in_sems.at[2 + PIECES]))
+    for read in reads:
+        read.start()
+
     barrier = pltpu.get_barrier_semaphore()
     for direction in range(4):
         @pl.when(exists[direction])
@@ -86,20 +97,26 @@
         def _():
             weights(phase, block, c, 0).wait_recv()
 
+    reads[0].wait()
+    gain[...] = jnp.transpose(jnp.broadcast_to(gain_row[...], (LANES, rows)))
+    always = z >= 0
     for c in range(PIECES):
+        reads[1 + c].wait()
         where = pl.ds(pl.multiple_of(me * rows + c * piece, piece), piece)
         part = slice(c * piece, (c + 1) * piece)
-        up_all[where, :] = (gain[part, :] * up_f[part, :]).astype(jnp.bfloat16)
-    pl.semaphore_wait(barrier, sum(e.astype(jnp.int32) for e in exists) + tp - 1)
-    always = z >= 0
-    for c in range(PIECES):
+        for k in range(0, width, LANES):
+            up_all[where, k:k + LANES] = (gain[part, :] * up_f[part, k:k + LANES]).astype(jnp.bfloat16)
+        if c == 0:
+            pl.semaphore_wait(barrier, sum(e.astype(jnp.int32) for e in exists) + tp - 1)
         for direction in range(4):
             send(always, 0, me, c, direction)
 
+    reads[1 + PIECES].wait()
     values = prompt[...].astype(jnp.float32)
     scale = lax.rsqrt(jnp.mean(values * values, axis=-1, keepdims=True) + 1e-06)
     mine = pl.ds(pl.multiple_of(t * tokens, tokens), tokens)
     norm_all[mine, :] = (values * scale).astype(jnp.bfloat16)
+    reads[2 + PIECES].wait()
     for c in range(PIECES):
         where = pl.ds(pl.multiple_of(me * rows + c * piece, piece), piece)
         part = slice(c * piece, (c + 1) * piece)
@@ -304,14 +321,20 @@
                 pltpu.VMEM(down_shape, bf16),
                 pltpu.VMEM((tokens, depth), bf16),
             ),
-            in_specs=[vmem] * 4,
+            in_specs=[any_space] * 4,
             out_specs=[vmem] * 3,
             scratch_shapes=[
+                pltpu.VMEM((tokens, depth), bf16),
+                pltpu.VMEM((1, rows), jnp.float32),
+                pltpu.VMEM((rows, LANES), jnp.float32),
+                pltpu.VMEM((rows, width), jnp.float32),
+                pltpu.VMEM((rows, width), jnp.float32),
                 pltpu.VMEM((depth, width) if turned else (16, 128), bf16),
                 pltpu.VMEM((tp * tokens, depth), bf16),
                 pltpu.VMEM((tp * tokens, width), bf16),
                 pltpu.VMEM((fs, tp * tokens, rows), bf16),
                 pltpu.VMEM((tp, fs, tokens, rows), bf16),
+                pltpu.SemaphoreType.DMA((3 + PIECES,)),
                 pltpu.SemaphoreType.DMA((4, slots)),
                 pltpu.SemaphoreType.DMA((slots,)),
                 pltpu.SemaphoreType.DMA((tp,)),
@@ -322,7 +345,7 @@
             compiler_params=pltpu.CompilerParams(
                 collective_id=0, has_side_effects=True, vmem_limit_bytes=LIMIT * 1024 * 1024
             ),
-        )(prompt, norm_gain[:, None], up_trained, down_trained)
+        )(prompt, norm_gain[None, :], up_trained, down_trained)
         up_whole, down_whole, mixed = pl.pallas_call(
             flush,
             out_shape=(

time: 183 us -> 179 us (0.978)
  Pallas kernels: 180 us -> 178 us
    pallas_call x1, Pallas kernels: 174 us -> 172 us  [shards(): pl.pallas_call(functools.partial(kernel, nz, ny, tp), out_shape=(pltpu.VM...]
where the time goes in v1:
time: 179 us
  Pallas kernels  178 us (99%)
    pallas_call x1, Pallas kernels, shards(): pl.pallas_call(functools.partial(kernel, nz, ny, tp), out_shape=(pltpu.VM...  172 us
    pallas_call x1, Pallas kernels, shards(): pl.pallas_call(flush, out_shape=(jax.ShapeDtypeStruct((depth, width), bf1...  6.19 us

profile of v1, /device:TPU:0, one launch (start us, length us, event | category | flops | bytes accessed | tf_op | source)
XLA Modules:
  0.0 178.8 jit_solution(4025804853334279569)
XLA Ops:
  0.6 171.9 %shard_map.67 = (bf16[2048,2048]{1,0:T(8,128)(2,1)S(1)}, bf16[2048,2048]{1,0:T(8,128)(2,1)S(1)}, bf16[128,2048]{1,0:T(8,128)(2,1)S(1)}) custom-call(bf16[128,2048]{1,0:T(8,128)(2,1)} %prompt_hbm.1, f32[1,256]{1,0:T(1,128)} %bitcast.1, f32[256,2048]{1,0:T(8,128)} %up_hbm.1, f32[256,2048]{1,0:T(8,128)} %down_hbm.1), custom_call_target="tpu_custom_call" | custom-call | tf_op jit(solution)/shard_map/pallas_call | solution.py:317
  172.6 6.2 %shard_map.68 = (bf16[2048,2048]{1,0:T(8,128)(2,1)}, bf16[2048,2048]{1,0:T(8,128)(2,1)}, bf16[128,2048]{1,0:T(8,128)(2,1)}) custom-call(bf16[2048,2048]{1,0:T(8,128)(2,1)S(1)} %get-tuple-element.6.up_in, bf16[2048,2048]{1,0:T(8,128)(2,1)S(1)} %get-tuple-element.7.down_in, bf16[128,2048]{1,0:T(8,128)(2,1)S(1)} %get-tuple-element.8.mixed_in), custom_call_target="tpu_custom_call" | custom-call | tf_op jit(solution)/shard_map/pallas_call | solution.py:349

commit v2 on v1

--- a/solution.py
+++ b/solution.py
@@ -22,6 +22,10 @@
 
 def turns(rows):
     return rows % 128 == 0
+
+
+def units_of(rows):
+    return PIECES if rows // PIECES % LANES == 0 else 1
 
 
 def flush(up_in, down_in, mixed_in, up_out, down_out, mixed_out, sems):
@@ -51,12 +55,11 @@
     z, y = me // ny, lax.rem(me, ny)
     exists = (z < nz - 1, z > 0, y < ny - 1, y > 0)
     step = (ny, -ny, 1, -1)
-    trick = ny == 2 and nz % 2 == 0
+    units = units_of(rows)
+    span = rows // units
+    trick = ny == 2 and nz > 2 and units == PIECES
     half = PIECES // 2
-    even = lax.rem(z, 2) == 0
-    mate = z + 1 - 2 * lax.rem(z, 2)
     buffers = (up_all, down_all)
-    sent = []
 
     reads = [pltpu.make_async_copy(gain_hbm, gain_row, in_sems.at[0])]
     for c in range(PIECES):
@@ -81,14 +84,11 @@
         slot = (phase * fs + block) * PIECES + c
         return pltpu.make_async_remote_copy(
             src_ref=ref, dst_ref=ref,
-            send_sem=w_send.at[direction, slot], recv_sem=w_recv.at[slot],
+            send_sem=w_send.at[direction, phase], recv_sem=w_recv.at[slot],
             device_id={"fs": me + step[direction]}, device_id_type=MESH)
 
     def send(condition, phase, block, c, direction):
-        condition = jnp.logical_and(condition, exists[direction])
-        sent.append((condition, phase, block, c, direction))
-
-        @pl.when(condition)
+        @pl.when(jnp.logical_and(condition, exists[direction]))
         def _():
             weights(phase, block, c, direction).start()
 
@@ -143,22 +143,41 @@
 
     def own_down(d):
         for c in range(PIECES):
+            if trick and c >= half and d == nz - 2:
+                continue
             send(z == d, 1, me, c, 0)
             send(z == nz - 1 - d, 1, me, c, 1)
 
+    def own_late():
+        if trick:
+            for c in range(half, PIECES):
+                send(z == nz - 2, 1, me, c, 0)
+                send(z == 1, 1, me, c, 1)
+
+    def own_aside():
+        for c in range(half, PIECES):
+            for direction in (2, 3):
+                send(always, 1, me, c, direction)
+
     def column(phase, d):
         for c in range(PIECES):
+            near = trick and c >= half and d == 1
             for s in (1, -1):
                 zb = z + s * d
                 there = jnp.logical_and(zb >= 0, zb < nz)
+                if near and phase == 1:
+                    there = jnp.logical_and(there, exists[1 if s > 0 else 0])
                 block = zb * ny + y
                 arrive(there, phase, block, c)
                 send(there, phase, block, c, 1 if s > 0 else 0)
-                across = there
-                if trick and c >= half:
-                    across = jnp.logical_and(there, zb != mate)
-                send(across, phase, block, c, 2)
-                send(across, phase, block, c, 3)
+                if not near:
+                    send(there, phase, block, c, 2)
+                    send(there, phase, block, c, 3)
+
+    def landed():
+        for c in range(half, PIECES):
+            arrive(z == 0, 1, (z + 1) * ny + y, c)
+            arrive(z == nz - 1, 1, (z - 1) * ny + y, c)
 
     def swap(phase):
         if not trick:
@@ -167,72 +186,122 @@
         for c in range(half, PIECES):
             if phase == 0:
                 arrive(always, phase, block, c)
-            send(even, phase, block, c, 0)
-            send(jnp.logical_not(even), phase, block, c, 1)
-
-    def sideways(phase, d, s):
+            send(always, phase, block, c, 0)
+            send(always, phase, block, c, 1)
+
+    def sideways(phase, d, s, pieces):
         zb = z + s * d
         inside = jnp.logical_and(zb >= 0, zb < nz)
         for e in range(1, ny):
             for u in (1, -1):
                 yb = y + u * e
                 there = jnp.logical_and(inside, jnp.logical_and(yb >= 0, yb < ny))
-                for c in range(PIECES):
-                    if trick and phase == 0 and d == 0 and c >= half:
+                for c in pieces:
+                    if trick and c >= half and (d == 1 or (phase == 0 and d == 0)):
                         continue
-                    wanted = there
-                    if trick and c >= half:
-                        wanted = jnp.logical_and(there, zb != mate)
-                    arrive(wanted, phase, zb * ny + yb, c)
+                    arrive(there, phase, zb * ny + yb, c)
                     if e < ny - 1:
-                        send(wanted, phase, zb * ny + yb, c, 3 if u > 0 else 2)
+                        send(there, phase, zb * ny + yb, c, 3 if u > 0 else 2)
 
     def swapped(phase):
         if trick:
             for c in range(half, PIECES):
-                arrive(always, phase, mate * ny + 1 - y, c)
-
-    def partial_copy(block, offset):
+                for s in (1, -1):
+                    zb = z + s
+                    arrive(jnp.logical_and(zb >= 0, zb < nz), phase, zb * ny + 1 - y, c)
+
+    def partial_copy(unit, offset, group):
         peer = lax.rem(t + offset, tp)
         return pltpu.make_async_remote_copy(
-            src_ref=part_send.at[block, pl.ds(pl.multiple_of(peer * tokens, tokens), tokens)],
-            dst_ref=part_recv.at[t, block],
-            send_sem=p_send.at[offset], recv_sem=p_recv.at[t],
+            src_ref=part_send.at[unit, pl.ds(pl.multiple_of(peer * tokens, tokens), tokens)],
+            dst_ref=part_recv.at[t, unit],
+            send_sem=p_send.at[offset], recv_sem=p_recv.at[t, group],
             device_id={"tp": peer}, device_id_type=MESH)
 
-    def consume(condition, block):
+    def arrivals(group, count):
+        for offset in range(1, tp):
+            source = lax.rem(t + offset, tp)
+            ref = part_recv.at[source, pl.ds(0, count)]
+            pltpu.make_async_remote_copy(
+                src_ref=ref, dst_ref=ref, send_sem=p_send.at[offset], recv_sem=p_recv.at[source, group],
+                device_id={"tp": source}, device_id_type=MESH).wait_recv()
+
+    def multiply(condition, block, u, group=0):
         @pl.when(condition)
         def _():
-            where = pl.ds(pl.multiple_of(block * rows, rows), rows)
-            part_send[block] = lax.dot_general(
+            where = pl.ds(pl.multiple_of(block * rows + u * span, span), span)
+            unit = block * units + u
+            part_send[unit] = lax.dot_general(
                 hidden[...], down_all[where, :], (((1,), (1,)), ((), ())),
                 preferred_element_type=jnp.float32).astype(jnp.bfloat16)
             for offset in range(1, tp):
-                partial_copy(block, offset).start()
-            if turned:
-                @pl.loop(0, width // tile)
-                def _(j):
-                    at = pl.ds(pl.multiple_of(j * tile, tile), tile)
-                    down_out[at, where] = jnp.transpose(down_all[where, at])
-
-    def consume_column(d):
-        @pl.loop(0, 1 if d == 0 else 2)
+                partial_copy(unit, offset, group).start()
+
+    def turn(condition, block, u):
+        if not turned:
+            return
+
+        @pl.when(condition)
+        def _():
+            where = pl.ds(pl.multiple_of(block * rows + u * span, span), span)
+
+            @pl.loop(0, width // tile)
+            def _(j):
+                at = pl.ds(pl.multiple_of(j * tile, tile), tile)
+                down_out[at, where] = jnp.transpose(down_all[where, at])
+
+    def consume(condition, block, u):
+        multiply(condition, block, u)
+        turn(condition, block, u)
+
+    def total_of(unit):
+        total = part_send[unit, mine, :].astype(jnp.float32)
+        for offset in range(1, tp):
+            total += part_recv[lax.rem(t + offset, tp), unit].astype(jnp.float32)
+        return total.astype(jnp.bfloat16)
+
+    def add(condition, block, u):
+        @pl.when(condition)
+        def _():
+            unit = block * units + u
+            mixed[:, pl.ds(pl.multiple_of(unit * span, span), span)] = total_of(unit)
+
+    def walk(action, d, aside, first, count):
+        across = ny - 1 if aside else 1
+        if across * count == 0:
+            return
+
+        @pl.loop(0, (1 if d == 0 else 2) * across * count)
         def _(i):
-            zb = z + (1 - 2 * i) * d
-            consume(jnp.logical_and(zb >= 0, zb < nz), zb * ny + y)
-
-    def consume_sideways(d):
-        @pl.loop(0, (1 if d == 0 else 2) * (ny - 1))
-        def _(i):
-            zb = z + (1 - 2 * (i // (ny - 1))) * d
-            yb = lax.rem(y + 1 + lax.rem(i, ny - 1), ny)
-            inside = jnp.logical_and(zb >= 0, zb < nz)
-            if trick:
-                inside = jnp.logical_and(inside, zb != mate)
-            consume(inside, zb * ny + yb)
+            k = i // count
+            zb = z + (1 - 2 * (k // across)) * d
+            yb = lax.rem(y + 1 + lax.rem(k, across), ny) if aside else y
+            action(jnp.logical_and(zb >= 0, zb < nz), zb * ny + yb, first + lax.rem(i, count))
+
+    pending = []
+
+    def use(*place):
+        walk(consume, *place)
+        pending.append(place)
+
+    def finish():
+        if span % LANES == 0:
+            for place in pending:
+                walk(add, *place)
+        pending.clear()
+
+    def use_aside(d, first, count):
+        for s in signs(d):
+            sideways(1, d, s, range(PIECES) if units == 1 else range(first, first + count))
+        use(d, True, first, count)
 
     def signs(d):
         return (1,) if d == 0 else (1, -1)
+
+    def ready(d):
+        use(d, False, 0, half if trick and d == 1 else units)
+        if d > 0:
+            use_aside(d - 1, 0, half if trick and d == 2 else units)
 
     own_down(0)
     for d in range(1, nz):
@@ -240,12 +309,15 @@
         if d == 1:
             swap(0)
         own_down(d)
-    for c in range(half, PIECES):
-        for direction in (2, 3):
-            send(always, 1, me, c, direction)
+        if d == nz // 2:
+            own_aside()
+    if nz == 1:
+        own_aside()
+    else:
+        column(1, 1)
     for d in range(nz):
         for s in signs(d):
-            sideways(0, d, s)
+            sideways(0, d, s, range(PIECES))
     swapped(0)
     for offset in range(1, tp):
         token_arrival(offset).wait_recv()
@@ -256,49 +328,73 @@
         pre = jnp.dot(norm_all[...], up_all[:, at], preferred_element_type=jnp.float32)
         hidden[:, at] = jnp.square(jnp.maximum(pre, 0.0)).astype(jnp.bfloat16)
 
-    for d in range(1, nz):
+    for d in range(min(nz, 2), nz):
         column(1, d)
         if d == nz - 1:
+            own_late()
             swap(1)
-        consume_column(d - 1)
-        if d == 1:
-            sideways(1, 0, 1)
-            consume_sideways(0)
-    if nz == 1:
-        sideways(1, 0, 1)
-        consume_sideways(0)
-    consume_column(nz - 1)
-    for d in range(1, nz):
-        for s in signs(d):
-            sideways(1, d, s)
-        consume_sideways(d)
+        if d == 2:
+            ready(0)
+            ready(1)
+        ready(d)
+    if nz <= 2:
+        for d in range(nz):
+            ready(d)
+    if trick:
+        landed()
+        use(1, False, half, units - half)
+    if units > 1:
+        use_aside(nz - 1, 0, units - 1)
+    late = 2 * (units - half) if trick else 0
+    ends = multiply
+    if trick:
+        arrivals(0, fs * units - late)
+        finish()
+        ends = functools.partial(multiply, group=1)
+    last = [(nz - 1, True, units - 1, 1)]
+    for s in signs(nz - 1):
+        sideways(1, nz - 1, s, range(PIECES) if units == 1 else range(units - 1, units))
+    walk(ends, *last[0])
     if trick:
         swapped(1)
-        consume(always, mate * ny + 1 - y)
-
-    for offset in range(1, tp):
-        source = lax.rem(t + offset, tp)
-        whole = part_recv.at[source]
-        arrival = pltpu.make_async_remote_copy(
-            src_ref=whole, dst_ref=whole, send_sem=p_send.at[offset], recv_sem=p_recv.at[source],
-            device_id={"tp": source}, device_id_type=MESH)
-        arrival.wait_recv()
-    for block in range(fs):
-        total = part_send[block, mine, :].astype(jnp.float32)
-        for offset in range(1, tp):
-            total += part_recv[lax.rem(t + offset, tp), block].astype(jnp.float32)
-        mixed[:, block * rows:(block + 1) * rows] = total.astype(jnp.bfloat16)
+        last.append((1, True, half, units - half))
+        walk(ends, *last[1])
+    for place in last:
+        walk(turn, *place)
+        pending.append(place)
+    arrivals(1 if trick else 0, late if trick else fs * units)
+    finish()
+    if span % LANES:
+        for block in range(fs):
+            mixed[:, block * rows:(block + 1) * rows] = total_of(block)
 
     for offset in range(1, tp):
         token_copy(offset).wait_send()
+
+    for offset in range(1, tp):
         whole = part_recv.at[t]
         pltpu.make_async_remote_copy(
-            src_ref=whole, dst_ref=whole, send_sem=p_send.at[offset], recv_sem=p_recv.at[t],
+            src_ref=whole, dst_ref=whole, send_sem=p_send.at[offset], recv_sem=p_recv.at[t, 0],
             device_id={"tp": lax.rem(t + offset, tp)}, device_id_type=MESH).wait_send()
-    for condition, phase, block, c, direction in sent:
-        @pl.when(condition)
-        def _():
-            weights(phase, block, c, direction).wait_send()
+
+    def drain(condition, direction, pieces):
+        @pl.when(jnp.logical_and(condition, exists[direction]))
+        def _():
+            for phase in range(2):
+                ref = buffers[phase].at[pl.ds(0, pieces * piece)]
+                pltpu.make_async_remote_copy(
+                    src_ref=ref, dst_ref=ref, send_sem=w_send.at[direction, phase], recv_sem=w_recv.at[0],
+                    device_id={"fs": me + step[direction]}, device_id_type=MESH).wait_send()
+
+    spare = PIECES - half if trick else 0
+    for k in range(nz):
+        drain(z == k, 0, (k + 1) * PIECES + spare)
+        drain(z == k, 1, (nz - k) * PIECES + spare)
+        less = spare * ((k > 0) + (k < nz - 1))
+        for e in range(ny):
+            here = jnp.logical_and(z == k, y == e)
+            drain(here, 2, (e + 1) * nz * PIECES - less)
+            drain(here, 3, (ny - e) * nz * PIECES - less)
 
 
 def solution(mesh):
@@ -312,6 +408,7 @@
         turned = turns(rows)
         down_shape = (width, depth) if turned else (depth, width)
         slots = 2 * fs * PIECES
+        parts = fs * units_of(rows)
         any_space = pl.BlockSpec(memory_space=pl.ANY)
         vmem = pl.BlockSpec(memory_space=pltpu.VMEM)
         up_whole, down_whole, mixed = pl.pallas_call(
@@ -332,15 +429,15 @@
                 pltpu.VMEM((depth, width) if turned else (16, 128), bf16),
                 pltpu.VMEM((tp * tokens, depth), bf16),
                 pltpu.VMEM((tp * tokens, width), bf16),
-                pltpu.VMEM((fs, tp * tokens, rows), bf16),
-                pltpu.VMEM((tp, fs, tokens, rows), bf16),
+                pltpu.VMEM((parts, tp * tokens, depth // parts), bf16),
+                pltpu.VMEM((tp, parts, tokens, depth // parts), bf16),
                 pltpu.SemaphoreType.DMA((3 + PIECES,)),
-                pltpu.SemaphoreType.DMA((4, slots)),
+                pltpu.SemaphoreType.DMA((4, 2)),
                 pltpu.SemaphoreType.DMA((slots,)),
                 pltpu.SemaphoreType.DMA((tp,)),
                 pltpu.SemaphoreType.DMA((tp,)),
                 pltpu.SemaphoreType.DMA((tp,)),
-                pltpu.SemaphoreType.DMA((tp,)),
+                pltpu.SemaphoreType.DMA((tp, 2)),
             ],
             compiler_params=pltpu.CompilerParams(
                 collective_id=0, has_side_effects=True, vmem_limit_bytes=LIMIT * 1024 * 1024

time: 179 us -> 175 us (0.978)
  Pallas kernels: 178 us -> 174 us
    pallas_call x1, Pallas kernels: 172 us -> 168 us  [shards(): pl.pallas_call(functools.partial(kernel, nz, ny, tp), out_shape=(pltpu.VM...]
where the time goes in v2:
time: 175 us
  Pallas kernels  174 us (99%)
    pallas_call x1, Pallas kernels, shards(): pl.pallas_call(functools.partial(kernel, nz, ny, tp), out_shape=(pltpu.VM...  168 us
    pallas_call x1, Pallas kernels, shards(): pl.pallas_call(flush, out_shape=(jax.ShapeDtypeStruct((depth, width), bf1...  6.19 us

profile of v2, /device:TPU:0, one launch (start us, length us, event | category | flops | bytes accessed | tf_op | source)
XLA Modules:
  0.0 174.8 jit_solution(13673976186904988403)
XLA Ops:
  0.6 168.0 %shard_map.67 = (bf16[2048,2048]{1,0:T(8,128)(2,1)S(1)}, bf16[2048,2048]{1,0:T(8,128)(2,1)S(1)}, bf16[128,2048]{1,0:T(8,128)(2,1)S(1)}) custom-call(bf16[128,2048]{1,0:T(8,128)(2,1)} %prompt_hbm.1, f32[1,256]{1,0:T(1,128)} %bitcast.1, f32[256,2048]{1,0:T(8,128)} %up_hbm.1, f32[256,2048]{1,0:T(8,128)} %down_hbm.1), custom_call_target="tpu_custom_call" | custom-call | tf_op jit(solution)/shard_map/pallas_call | solution.py:414
  168.6 6.2 %shard_map.68 = (bf16[2048,2048]{1,0:T(8,128)(2,1)}, bf16[2048,2048]{1,0:T(8,128)(2,1)}, bf16[128,2048]{1,0:T(8,128)(2,1)}) custom-call(bf16[2048,2048]{1,0:T(8,128)(2,1)S(1)} %get-tuple-element.6.up_in, bf16[2048,2048]{1,0:T(8,128)(2,1)S(1)} %get-tuple-element.7.down_in, bf16[128,2048]{1,0:T(8,128)(2,1)S(1)} %get-tuple-element.8.mixed_in), custom_call_target="tpu_custom_call" | custom-call | tf_op jit(solution)/shard_map/pallas_call | solution.py:446

commit v3 on v2

--- a/solution.py
+++ b/solution.py
@@ -11,6 +11,8 @@
 PIECES = 2
 LIMIT = 40
 LANES = 128
+CUTS = 4
+TURN = 128 * 1024
 
 
 def factor(fs):
@@ -41,8 +43,8 @@
 
 def kernel(nz, ny, tp, prompt_hbm, gain_hbm, up_hbm, down_hbm, up_all, down_out, mixed,
            prompt, gain_row, gain, up_f, down_f,
-           down_scratch, norm_all, hidden, part_send, part_recv,
-           in_sems, w_send, w_recv, n_send, n_recv, p_send, p_recv):
+           down_scratch, norm_all, hidden, part_send, part_recv, late_send, late_recv,
+           in_sems, w_send, w_recv, w_late, n_send, n_recv, p_send, p_recv):
     fs = nz * ny
     rows, width = up_f.shape
     tile = 256
@@ -57,17 +59,21 @@
     step = (ny, -ny, 1, -1)
     units = units_of(rows)
     span = rows // units
-    trick = ny == 2 and nz > 2 and units == PIECES
+    trick = ny == 2 and nz > 2 and units == PIECES == 2 and tokens % LANES == 0
+    cut = piece // CUTS
+    opening = CUTS if cut % 16 == 0 else 1
     half = PIECES // 2
     buffers = (up_all, down_all)
 
+    bounds = [(k * piece // opening, piece // opening) for k in range(opening)]
+    bounds += [(c * piece, piece) for c in range(1, PIECES)]
     reads = [pltpu.make_async_copy(gain_hbm, gain_row, in_sems.at[0])]
-    for c in range(PIECES):
-        part = pl.ds(c * piece, piece)
-        reads.append(pltpu.make_async_copy(up_hbm.at[part], up_f.at[part], in_sems.at[1 + c]))
-    reads.append(pltpu.make_async_copy(prompt_hbm, prompt, in_sems.at[1 + PIECES]))
-    reads.append(pltpu.make_async_copy(down_hbm, down_f, in_sems.at[2 + PIECES]))
-    for read in reads:
+    for k, (start, size) in enumerate(bounds):
+        part = pl.ds(start, size)
+        reads.append(pltpu.make_async_copy(up_hbm.at[part], up_f.at[part], in_sems.at[1 + k]))
+    reads.append(pltpu.make_async_copy(prompt_hbm, prompt, in_sems.at[1 + len(bounds)]))
+    reads.append(pltpu.make_async_copy(down_hbm, down_f, in_sems.at[2 + len(bounds)]))
+    for read in reads[:1 + opening]:
         read.start()
 
     barrier = pltpu.get_barrier_semaphore()
@@ -78,14 +84,23 @@
     for offset in range(1, tp):
         pl.semaphore_signal(barrier, inc=1, device_id={"tp": lax.rem(t + offset, tp)}, device_id_type=MESH)
 
-    def weights(phase, block, c, direction):
-        start = pl.multiple_of(block * rows + c * piece, piece)
-        ref = buffers[phase].at[pl.ds(start, piece)]
-        slot = (phase * fs + block) * PIECES + c
+    def rows_copy(phase, start, size, direction, landing):
+        ref = buffers[phase].at[pl.ds(pl.multiple_of(start, size), size)]
         return pltpu.make_async_remote_copy(
             src_ref=ref, dst_ref=ref,
-            send_sem=w_send.at[direction, phase], recv_sem=w_recv.at[slot],
+            send_sem=w_send.at[direction, phase], recv_sem=landing,
             device_id={"fs": me + step[direction]}, device_id_type=MESH)
+
+    def weights(phase, block, c, direction):
+        slot = (phase * fs + block) * PIECES + c
+        return rows_copy(phase, block * rows + c * piece, piece, direction, w_recv.at[slot])
+
+    def send_late(condition, block, direction, kind):
+        @pl.when(jnp.logical_and(condition, exists[direction]))
+        def _():
+            for k in range(CUTS):
+                start = block * rows + half * piece + k * cut
+                rows_copy(1, start, cut, direction, w_late.at[kind, k]).start()
 
     def send(condition, phase, block, c, direction):
         @pl.when(jnp.logical_and(condition, exists[direction]))
@@ -100,23 +115,28 @@
     reads[0].wait()
     gain[...] = jnp.transpose(jnp.broadcast_to(gain_row[...], (LANES, rows)))
     always = z >= 0
-    for c in range(PIECES):
-        reads[1 + c].wait()
-        where = pl.ds(pl.multiple_of(me * rows + c * piece, piece), piece)
-        part = slice(c * piece, (c + 1) * piece)
-        for k in range(0, width, LANES):
-            up_all[where, k:k + LANES] = (gain[part, :] * up_f[part, k:k + LANES]).astype(jnp.bfloat16)
-        if c == 0:
+    for k, (start, size) in enumerate(bounds):
+        reads[1 + k].wait()
+        if k == opening - 1:
+            for read in reads[1 + opening:]:
+                read.start()
+        where = pl.ds(pl.multiple_of(me * rows + start, size), size)
+        for n in range(0, width, LANES):
+            up_all[where, n:n + LANES] = (
+                gain[start:start + size, :] * up_f[start:start + size, n:n + LANES]).astype(jnp.bfloat16)
+        if k == 0:
             pl.semaphore_wait(barrier, sum(e.astype(jnp.int32) for e in exists) + tp - 1)
         for direction in range(4):
-            send(always, 0, me, c, direction)
-
-    reads[1 + PIECES].wait()
+            @pl.when(exists[direction])
+            def _():
+                rows_copy(0, me * rows + start, size, direction, w_recv.at[me * PIECES + start // piece]).start()
+
+    reads[1 + len(bounds)].wait()
     values = prompt[...].astype(jnp.float32)
     scale = lax.rsqrt(jnp.mean(values * values, axis=-1, keepdims=True) + 1e-06)
     mine = pl.ds(pl.multiple_of(t * tokens, tokens), tokens)
     norm_all[mine, :] = (values * scale).astype(jnp.bfloat16)
-    reads[2 + PIECES].wait()
+    reads[2 + len(bounds)].wait()
     for c in range(PIECES):
         where = pl.ds(pl.multiple_of(me * rows + c * piece, piece), piece)
         part = slice(c * piece, (c + 1) * piece)
@@ -170,7 +190,10 @@
                 block = zb * ny + y
                 arrive(there, phase, block, c)
                 send(there, phase, block, c, 1 if s > 0 else 0)
-                if not near:
+                if trick and phase == 1 and d == nz - 1 and c >= half:
+                    send_late(there, block, 2, 0)
+                    send_late(there, block, 3, 0)
+                elif not near:
                     send(there, phase, block, c, 2)
                     send(there, phase, block, c, 3)
 
@@ -186,8 +209,11 @@
         for c in range(half, PIECES):
             if phase == 0:
                 arrive(always, phase, block, c)
-            send(always, phase, block, c, 0)
-            send(always, phase, block, c, 1)
+                send(always, phase, block, c, 0)
+                send(always, phase, block, c, 1)
+            else:
+                send_late(always, block, 0, 2)
+                send_late(always, block, 1, 1)
 
     def sideways(phase, d, s, pieces):
         zb = z + s * d
@@ -210,49 +236,53 @@
                     zb = z + s
                     arrive(jnp.logical_and(zb >= 0, zb < nz), phase, zb * ny + 1 - y, c)
 
-    def partial_copy(unit, offset, group):
+    def partial_copy(unit, count, offset):
         peer = lax.rem(t + offset, tp)
         return pltpu.make_async_remote_copy(
-            src_ref=part_send.at[unit, pl.ds(pl.multiple_of(peer * tokens, tokens), tokens)],
-            dst_ref=part_recv.at[t, unit],
-            send_sem=p_send.at[offset], recv_sem=p_recv.at[t, group],
+            src_ref=part_send.at[pl.ds(unit, count), pl.ds(pl.multiple_of(peer * tokens, tokens), tokens)],
+            dst_ref=part_recv.at[t, pl.ds(unit, count)],
+            send_sem=p_send.at[offset], recv_sem=p_recv.at[t, 0],
             device_id={"tp": peer}, device_id_type=MESH)
 
-    def arrivals(group, count):
+    def arrivals(count):
         for offset in range(1, tp):
             source = lax.rem(t + offset, tp)
             ref = part_recv.at[source, pl.ds(0, count)]
             pltpu.make_async_remote_copy(
-                src_ref=ref, dst_ref=ref, send_sem=p_send.at[offset], recv_sem=p_recv.at[source, group],
+                src_ref=ref, dst_ref=ref, send_sem=p_send.at[offset], recv_sem=p_recv.at[source, 0],
                 device_id={"tp": source}, device_id_type=MESH).wait_recv()
 
-    def multiply(condition, block, u, group=0):
+    def multiply(condition, block, u, count):
         @pl.when(condition)
         def _():
-            where = pl.ds(pl.multiple_of(block * rows + u * span, span), span)
+            where = pl.ds(pl.multiple_of(block * rows + u * span, span), count * span)
             unit = block * units + u
-            part_send[unit] = lax.dot_general(
+            product = lax.dot_general(
                 hidden[...], down_all[where, :], (((1,), (1,)), ((), ())),
                 preferred_element_type=jnp.float32).astype(jnp.bfloat16)
+            for k in range(count):
+                part_send[unit + k] = product[:, k * span:(k + 1) * span]
             for offset in range(1, tp):
-                partial_copy(unit, offset, group).start()
-
-    def turn(condition, block, u):
+                partial_copy(unit, count, offset).start()
+
+    def turn(condition, block, u, count):
         if not turned:
             return
+        deep = count * span
+        wide = TURN // deep if width % (TURN // deep) == 0 else tile
 
         @pl.when(condition)
         def _():
-            where = pl.ds(pl.multiple_of(block * rows + u * span, span), span)
-
-            @pl.loop(0, width // tile)
+            where = pl.ds(pl.multiple_of(block * rows + u * span, span), deep)
+
+            @pl.loop(0, width // wide)
             def _(j):
-                at = pl.ds(pl.multiple_of(j * tile, tile), tile)
+                at = pl.ds(pl.multiple_of(j * wide, wide), wide)
                 down_out[at, where] = jnp.transpose(down_all[where, at])
 
-    def consume(condition, block, u):
-        multiply(condition, block, u)
-        turn(condition, block, u)
+    def consume(condition, block, u, count):
+        multiply(condition, block, u, count)
+        turn(condition, block, u, count)
 
     def total_of(unit):
         total = part_send[unit, mine, :].astype(jnp.float32)
@@ -260,23 +290,23 @@
             total += part_recv[lax.rem(t + offset, tp), unit].astype(jnp.float32)
         return total.astype(jnp.bfloat16)
 
-    def add(condition, block, u):
+    def add(condition, block, u, count):
         @pl.when(condition)
         def _():
-            unit = block * units + u
-            mixed[:, pl.ds(pl.multiple_of(unit * span, span), span)] = total_of(unit)
+            for k in range(count):
+                unit = block * units + u + k
+                mixed[:, pl.ds(pl.multiple_of(unit * span, span), span)] = total_of(unit)
 
     def walk(action, d, aside, first, count):
         across = ny - 1 if aside else 1
         if across * count == 0:
             return
 
-        @pl.loop(0, (1 if d == 0 else 2) * across * count)
-        def _(i):
-            k = i // count
+        @pl.loop(0, (1 if d == 0 else 2) * across)
+        def _(k):
             zb = z + (1 - 2 * (k // across)) * d
             yb = lax.rem(y + 1 + lax.rem(k, across), ny) if aside else y
-            action(jnp.logical_and(zb >= 0, zb < nz), zb * ny + yb, first + lax.rem(i, count))
+            action(jnp.logical_and(zb >= 0, zb < nz), zb * ny + yb, first, count)
 
     pending = []
 
@@ -345,25 +375,59 @@
         use(1, False, half, units - half)
     if units > 1:
         use_aside(nz - 1, 0, units - 1)
-    late = 2 * (units - half) if trick else 0
-    ends = multiply
     if trick:
-        arrivals(0, fs * units - late)
+        arrivals(fs * units - 2)
         finish()
-        ends = functools.partial(multiply, group=1)
-    last = [(nz - 1, True, units - 1, 1)]
-    for s in signs(nz - 1):
-        sideways(1, nz - 1, s, range(PIECES) if units == 1 else range(units - 1, units))
-    walk(ends, *last[0])
-    if trick:
-        swapped(1)
-        last.append((1, True, half, units - half))
-        walk(ends, *last[1])
-    for place in last:
-        walk(turn, *place)
-        pending.append(place)
-    arrivals(1 if trick else 0, late if trick else fs * units)
-    finish()
+        lowest, highest = (z == 0).astype(jnp.int32), (z == nz - 1).astype(jnp.int32)
+        inner = 1 - lowest - highest
+
+        def late(slot):
+            first = lowest * (nz - 1) + inner * (z - 1)
+            block = (first + slot * (z + 1 - 2 * highest - first)) * ny + 1 - y
+            return block, 2 * inner + slot * (1 + highest - 2 * inner)
+
+        @pl.loop(0, CUTS)
+        def _(k):
+            here = pl.ds(pl.multiple_of(k * cut, cut), cut)
+            fresh = []
+            for slot in range(2):
+                block, kind = late(slot)
+                start = pl.multiple_of(block * rows + half * piece + k * cut, cut)
+                rows_copy(1, start, cut, 0, w_late.at[kind, k]).wait_recv()
+                fresh.append(down_all[pl.ds(start, cut), :])
+            product = jnp.transpose(lax.dot_general(
+                hidden[...], jnp.concatenate(fresh), (((1,), (1,)), ((), ())),
+                preferred_element_type=jnp.float32)).astype(jnp.bfloat16)
+            for slot in range(2):
+                late_send[slot, here, :] = product[slot * cut:(slot + 1) * cut]
+            for offset in range(tp - 1, 0, -1):
+                peer = lax.rem(t + offset, tp)
+                pltpu.make_async_remote_copy(
+                    src_ref=late_send.at[:, here, pl.ds(pl.multiple_of(peer * tokens, tokens), tokens)],
+                    dst_ref=late_recv.at[t, :, here],
+                    send_sem=p_send.at[offset], recv_sem=p_recv.at[t, 1],
+                    device_id={"tp": peer}, device_id_type=MESH).start()
+
+        for slot in range(2):
+            turn(always, late(slot)[0], half, 1)
+        for offset in range(1, tp):
+            source = lax.rem(t + offset, tp)
+            ref = late_recv.at[source]
+            pltpu.make_async_remote_copy(
+                src_ref=ref, dst_ref=ref, send_sem=p_send.at[offset], recv_sem=p_recv.at[source, 1],
+                device_id={"tp": source}, device_id_type=MESH).wait_recv()
+        for slot in range(2):
+            total = late_send[slot, :, mine].astype(jnp.float32)
+            for offset in range(1, tp):
+                total += late_recv[lax.rem(t + offset, tp), slot].astype(jnp.float32)
+            column_of = pl.multiple_of(late(slot)[0] * rows + half * piece, piece)
+            mixed[:, pl.ds(column_of, piece)] = jnp.transpose(total).astype(jnp.bfloat16)
+    else:
+        for s in signs(nz - 1):
+            sideways(1, nz - 1, s, range(PIECES) if units == 1 else range(units - 1, units))
+        use(nz - 1, True, units - 1, 1)
+        arrivals(fs * units)
+        finish()
     if span % LANES:
         for block in range(fs):
             mixed[:, block * rows:(block + 1) * rows] = total_of(block)
@@ -431,9 +495,12 @@
                 pltpu.VMEM((tp * tokens, width), bf16),
                 pltpu.VMEM((parts, tp * tokens, depth // parts), bf16),
                 pltpu.VMEM((tp, parts, tokens, depth // parts), bf16),
-                pltpu.SemaphoreType.DMA((3 + PIECES,)),
+                pltpu.VMEM((2, rows // PIECES, tp * tokens), bf16),
+                pltpu.VMEM((tp, 2, rows // PIECES, tokens), bf16),
+                pltpu.SemaphoreType.DMA((2 + CUTS + PIECES,)),
                 pltpu.SemaphoreType.DMA((4, 2)),
                 pltpu.SemaphoreType.DMA((slots,)),
+                pltpu.SemaphoreType.DMA((3, CUTS)),
                 pltpu.SemaphoreType.DMA((tp,)),
                 pltpu.SemaphoreType.DMA((tp,)),
                 pltpu.SemaphoreType.DMA((tp,)),

time: 175 us -> 174 us (level)
  no operation moved by 1% of the time
where the time goes in v3:
time: 174 us
  Pallas kernels  174 us (100%)
    pallas_call x1, Pallas kernels, shards(): pl.pallas_call(functools.partial(kernel, nz, ny, tp), out_shape=(pltpu.VM...  167 us
    pallas_call x1, Pallas kernels, shards(): pl.pallas_call(flush, out_shape=(jax.ShapeDtypeStruct((depth, width), bf1...  6.19 us

profile of v3, /device:TPU:0, one launch (start us, length us, event | category | flops | bytes accessed | tf_op | source)
XLA Modules:
  0.0 174.2 jit_solution(5576432665235563448)
XLA Ops:
  0.6 167.4 %shard_map.67 = (bf16[2048,2048]{1,0:T(8,128)(2,1)S(1)}, bf16[2048,2048]{1,0:T(8,128)(2,1)S(1)}, bf16[128,2048]{1,0:T(8,128)(2,1)S(1)}) custom-call(bf16[128,2048]{1,0:T(8,128)(2,1)} %prompt_hbm.1, f32[1,256]{1,0:T(1,128)} %bitcast.1, f32[256,2048]{1,0:T(8,128)} %up_hbm.1, f32[256,2048]{1,0:T(8,128)} %down_hbm.1), custom_call_target="tpu_custom_call" | custom-call | tf_op jit(solution)/shard_map/pallas_call | solution.py:478
  168.0 6.2 %shard_map.68 = (bf16[2048,2048]{1,0:T(8,128)(2,1)}, bf16[2048,2048]{1,0:T(8,128)(2,1)}, bf16[128,2048]{1,0:T(8,128)(2,1)}) custom-call(bf16[2048,2048]{1,0:T(8,128)(2,1)S(1)} %get-tuple-element.6.up_in, bf16[2048,2048]{1,0:T(8,128)(2,1)S(1)} %get-tuple-element.7.down_in, bf16[128,2048]{1,0:T(8,128)(2,1)S(1)} %get-tuple-element.8.mixed_in), custom_call_target="tpu_custom_call" | custom-call | tf_op jit(solution)/shard_map/pallas_call | solution.py:513

commit v4 on v3

--- a/solution.py
+++ b/solution.py
@@ -11,7 +11,8 @@
 PIECES = 2
 LIMIT = 40
 LANES = 128
-CUTS = 4
+CUTS = 8
+FLUSHES = 4
 TURN = 128 * 1024
 
 
@@ -31,10 +32,12 @@
 
 
 def flush(up_in, down_in, mixed_in, up_out, down_out, mixed_out, sems):
-    copies = [
-        pltpu.make_async_copy(source, target, sems.at[i])
-        for i, (source, target) in enumerate(((up_in, up_out), (down_in, down_out), (mixed_in, mixed_out)))
-    ]
+    copies = []
+    for i, (source, target) in enumerate(((up_in, up_out), (down_in, down_out), (mixed_in, mixed_out))):
+        deep = source.shape[0] // FLUSHES
+        for k in range(FLUSHES):
+            part = pl.ds(k * deep, deep)
+            copies.append(pltpu.make_async_copy(source.at[part], target.at[part], sems.at[i * FLUSHES + k]))
     for copy in copies:
         copy.start()
     for copy in copies:
@@ -44,7 +47,7 @@
 def kernel(nz, ny, tp, prompt_hbm, gain_hbm, up_hbm, down_hbm, up_all, down_out, mixed,
            prompt, gain_row, gain, up_f, down_f,
            down_scratch, norm_all, hidden, part_send, part_recv, late_send, late_recv,
-           in_sems, w_send, w_recv, w_late, n_send, n_recv, p_send, p_recv):
+           in_sems, w_send, w_recv, w_late, joint):
     fs = nz * ny
     rows, width = up_f.shape
     tile = 256
@@ -65,7 +68,8 @@
     half = PIECES // 2
     buffers = (up_all, down_all)
 
-    bounds = [(k * piece // opening, piece // opening) for k in range(opening)]
+    share = piece // opening
+    bounds = [(k * share, share) for k in range(opening)]
     bounds += [(c * piece, piece) for c in range(1, PIECES)]
     reads = [pltpu.make_async_copy(gain_hbm, gain_row, in_sems.at[0])]
     for k, (start, size) in enumerate(bounds):
@@ -129,7 +133,7 @@
         for direction in range(4):
             @pl.when(exists[direction])
             def _():
-                rows_copy(0, me * rows + start, size, direction, w_recv.at[me * PIECES + start // piece]).start()
+                rows_copy(0, me * rows + start, size, direction, w_recv.at[me * PIECES + max(0, k + 1 - opening)]).start()
 
     reads[1 + len(bounds)].wait()
     values = prompt[...].astype(jnp.float32)
@@ -145,15 +149,16 @@
     def token_copy(offset):
         return pltpu.make_async_remote_copy(
             src_ref=norm_all.at[mine], dst_ref=norm_all.at[mine],
-            send_sem=n_send.at[offset], recv_sem=n_recv.at[t],
+            send_sem=joint.at[0], recv_sem=joint.at[1],
             device_id={"tp": lax.rem(t + offset, tp)}, device_id_type=MESH)
 
-    def token_arrival(offset):
-        source = lax.rem(t + offset, tp)
-        ref = norm_all.at[pl.ds(pl.multiple_of(source * tokens, tokens), tokens)]
+    def settle(ref, sent, landed_on):
         return pltpu.make_async_remote_copy(
-            src_ref=ref, dst_ref=ref, send_sem=n_send.at[offset], recv_sem=n_recv.at[source],
-            device_id={"tp": source}, device_id_type=MESH)
+            src_ref=ref, dst_ref=ref, send_sem=joint.at[sent], recv_sem=joint.at[landed_on],
+            device_id={"tp": lax.rem(t + 1, tp)}, device_id_type=MESH)
+
+    peers = pl.ds(0, tp - 1)
+    tokens_of_peers = norm_all.at[pl.ds(0, (tp - 1) * tokens)]
 
     for offset in range(1, tp):
         token_copy(offset).start()
@@ -241,16 +246,11 @@
         return pltpu.make_async_remote_copy(
             src_ref=part_send.at[pl.ds(unit, count), pl.ds(pl.multiple_of(peer * tokens, tokens), tokens)],
             dst_ref=part_recv.at[t, pl.ds(unit, count)],
-            send_sem=p_send.at[offset], recv_sem=p_recv.at[t, 0],
+            send_sem=joint.at[2], recv_sem=joint.at[3],
             device_id={"tp": peer}, device_id_type=MESH)
 
     def arrivals(count):
-        for offset in range(1, tp):
-            source = lax.rem(t + offset, tp)
-            ref = part_recv.at[source, pl.ds(0, count)]
-            pltpu.make_async_remote_copy(
-                src_ref=ref, dst_ref=ref, send_sem=p_send.at[offset], recv_sem=p_recv.at[source, 0],
-                device_id={"tp": source}, device_id_type=MESH).wait_recv()
+        settle(part_recv.at[peers, pl.ds(0, count)], 2, 3).wait_recv()
 
     def multiply(condition, block, u, count):
         @pl.when(condition)
@@ -349,8 +349,7 @@
         for s in signs(d):
             sideways(0, d, s, range(PIECES))
     swapped(0)
-    for offset in range(1, tp):
-        token_arrival(offset).wait_recv()
+    settle(tokens_of_peers, 0, 1).wait_recv()
 
     @pl.loop(0, width // tile)
     def _(j):
@@ -405,17 +404,12 @@
                 pltpu.make_async_remote_copy(
                     src_ref=late_send.at[:, here, pl.ds(pl.multiple_of(peer * tokens, tokens), tokens)],
                     dst_ref=late_recv.at[t, :, here],
-                    send_sem=p_send.at[offset], recv_sem=p_recv.at[t, 1],
+                    send_sem=joint.at[2], recv_sem=joint.at[4],
                     device_id={"tp": peer}, device_id_type=MESH).start()
 
         for slot in range(2):
             turn(always, late(slot)[0], half, 1)
-        for offset in range(1, tp):
-            source = lax.rem(t + offset, tp)
-            ref = late_recv.at[source]
-            pltpu.make_async_remote_copy(
-                src_ref=ref, dst_ref=ref, send_sem=p_send.at[offset], recv_sem=p_recv.at[source, 1],
-                device_id={"tp": source}, device_id_type=MESH).wait_recv()
+        settle(late_recv.at[peers], 2, 4).wait_recv()
         for slot in range(2):
             total = late_send[slot, :, mine].astype(jnp.float32)
             for offset in range(1, tp):
@@ -432,33 +426,27 @@
         for block in range(fs):
             mixed[:, block * rows:(block + 1) * rows] = total_of(block)
 
-    for offset in range(1, tp):
-        token_copy(offset).wait_send()
-
-    for offset in range(1, tp):
-        whole = part_recv.at[t]
-        pltpu.make_async_remote_copy(
-            src_ref=whole, dst_ref=whole, send_sem=p_send.at[offset], recv_sem=p_recv.at[t, 0],
-            device_id={"tp": lax.rem(t + offset, tp)}, device_id_type=MESH).wait_send()
-
-    def drain(condition, direction, pieces):
+    settle(tokens_of_peers, 0, 1).wait_send()
+    settle(part_recv.at[peers], 2, 3).wait_send()
+
+    def drain(condition, direction, blocks, pieces):
         @pl.when(jnp.logical_and(condition, exists[direction]))
         def _():
             for phase in range(2):
-                ref = buffers[phase].at[pl.ds(0, pieces * piece)]
+                count = blocks * rows + (pieces * piece if trick else 0)
+                ref = buffers[phase].at[pl.ds(0, count)]
                 pltpu.make_async_remote_copy(
                     src_ref=ref, dst_ref=ref, send_sem=w_send.at[direction, phase], recv_sem=w_recv.at[0],
                     device_id={"fs": me + step[direction]}, device_id_type=MESH).wait_send()
 
-    spare = PIECES - half if trick else 0
     for k in range(nz):
-        drain(z == k, 0, (k + 1) * PIECES + spare)
-        drain(z == k, 1, (nz - k) * PIECES + spare)
-        less = spare * ((k > 0) + (k < nz - 1))
+        drain(z == k, 0, k + 1, 1)
+        drain(z == k, 1, nz - k, 1)
+        near = (k > 0) + (k < nz - 1)
         for e in range(ny):
             here = jnp.logical_and(z == k, y == e)
-            drain(here, 2, (e + 1) * nz * PIECES - less)
-            drain(here, 3, (ny - e) * nz * PIECES - less)
+            drain(here, 2, (e + 1) * nz, -near)
+            drain(here, 3, (ny - e) * nz, -near)
 
 
 def solution(mesh):
@@ -501,10 +489,7 @@
                 pltpu.SemaphoreType.DMA((4, 2)),
                 pltpu.SemaphoreType.DMA((slots,)),
                 pltpu.SemaphoreType.DMA((3, CUTS)),
-                pltpu.SemaphoreType.DMA((tp,)),
-                pltpu.SemaphoreType.DMA((tp,)),
-                pltpu.SemaphoreType.DMA((tp,)),
-                pltpu.SemaphoreType.DMA((tp, 2)),
+                pltpu.SemaphoreType.DMA((5,)),
             ],
             compiler_params=pltpu.CompilerParams(
                 collective_id=0, has_side_effects=True, vmem_limit_bytes=LIMIT * 1024 * 1024
@@ -519,7 +504,7 @@
             ),
             in_specs=[vmem] * 3,
             out_specs=[any_space] * 3,
-            scratch_shapes=[pltpu.SemaphoreType.DMA((3,))],
+            scratch_shapes=[pltpu.SemaphoreType.DMA((3 * FLUSHES,))],
             compiler_params=pltpu.CompilerParams(vmem_limit_bytes=2 * 1024 * 1024),
         )(up_whole, down_whole, mixed)
         return up_whole, down_whole if turned else jnp.transpose(down_whole), mixed

time: 174 us -> 174 us (level)
  no operation moved by 1% of the time
where the time goes in v4:
time: 174 us
  Pallas kernels  173 us (99%)
    pallas_call x1, Pallas kernels, shards(): pl.pallas_call(functools.partial(kernel, nz, ny, tp), out_shape=(pltpu.VM...  167 us
    pallas_call x1, Pallas kernels, shards(): pl.pallas_call(flush, out_shape=(jax.ShapeDtypeStruct((depth, width), bf1...  6.05 us

profile of v4, /device:TPU:0, one launch (start us, length us, event | category | flops | bytes accessed | tf_op | source)
XLA Modules:
  0.0 174.0 jit_solution(16665003737114693866)
XLA Ops:
  0.6 167.3 %shard_map.67 = (bf16[2048,2048]{1,0:T(8,128)(2,1)S(1)}, bf16[2048,2048]{1,0:T(8,128)(2,1)S(1)}, bf16[128,2048]{1,0:T(8,128)(2,1)S(1)}) custom-call(bf16[128,2048]{1,0:T(8,128)(2,1)} %prompt_hbm.1, f32[1,256]{1,0:T(1,128)} %bitcast.1, f32[256,2048]{1,0:T(8,128)} %up_hbm.1, f32[256,2048]{1,0:T(8,128)} %down_hbm.1), custom_call_target="tpu_custom_call" | custom-call | tf_op jit(solution)/shard_map/pallas_call | solution.py:466
  167.9 6.0 %shard_map.68 = (bf16[2048,2048]{1,0:T(8,128)(2,1)}, bf16[2048,2048]{1,0:T(8,128)(2,1)}, bf16[128,2048]{1,0:T(8,128)(2,1)}) custom-call(bf16[2048,2048]{1,0:T(8,128)(2,1)S(1)} %get-tuple-element.6.up_in, bf16[2048,2048]{1,0:T(8,128)(2,1)S(1)} %get-tuple-element.7.down_in, bf16[128,2048]{1,0:T(8,128)(2,1)S(1)} %get-tuple-element.8.mixed_in), custom_call_target="tpu_custom_call" | custom-call | tf_op jit(solution)/shard_map/pallas_call | solution.py:498

commit v5 on v4

--- a/solution.py
+++ b/solution.py
@@ -12,6 +12,7 @@
 LIMIT = 40
 LANES = 128
 CUTS = 8
+OPENING = 4
 FLUSHES = 4
 TURN = 128 * 1024
 
@@ -64,7 +65,7 @@
     span = rows // units
     trick = ny == 2 and nz > 2 and units == PIECES == 2 and tokens % LANES == 0
     cut = piece // CUTS
-    opening = CUTS if cut % 16 == 0 else 1
+    opening = OPENING if piece % (16 * OPENING) == 0 else 1
     half = PIECES // 2
     buffers = (up_all, down_all)
 
@@ -217,7 +218,7 @@
                 send(always, phase, block, c, 0)
                 send(always, phase, block, c, 1)
             else:
-                send_late(always, block, 0, 2)
+                send_late(always, block, 0, (z == nz - 2).astype(jnp.int32))
                 send_late(always, block, 1, 1)
 
     def sideways(phase, d, s, pieces):
@@ -383,16 +384,16 @@
         def late(slot):
             first = lowest * (nz - 1) + inner * (z - 1)
             block = (first + slot * (z + 1 - 2 * highest - first)) * ny + 1 - y
-            return block, 2 * inner + slot * (1 + highest - 2 * inner)
+            return block
 
         @pl.loop(0, CUTS)
         def _(k):
             here = pl.ds(pl.multiple_of(k * cut, cut), cut)
             fresh = []
             for slot in range(2):
-                block, kind = late(slot)
+                block = late(slot)
                 start = pl.multiple_of(block * rows + half * piece + k * cut, cut)
-                rows_copy(1, start, cut, 0, w_late.at[kind, k]).wait_recv()
+                rows_copy(1, start, cut, 0, w_late.at[slot, k]).wait_recv()
                 fresh.append(down_all[pl.ds(start, cut), :])
             product = jnp.transpose(lax.dot_general(
                 hidden[...], jnp.concatenate(fresh), (((1,), (1,)), ((), ())),
@@ -408,13 +409,13 @@
                     device_id={"tp": peer}, device_id_type=MESH).start()
 
         for slot in range(2):
-            turn(always, late(slot)[0], half, 1)
+            turn(always, late(slot), half, 1)
         settle(late_recv.at[peers], 2, 4).wait_recv()
         for slot in range(2):
             total = late_send[slot, :, mine].astype(jnp.float32)
             for offset in range(1, tp):
                 total += late_recv[lax.rem(t + offset, tp), slot].astype(jnp.float32)
-            column_of = pl.multiple_of(late(slot)[0] * rows + half * piece, piece)
+            column_of = pl.multiple_of(late(slot) * rows + half * piece, piece)
             mixed[:, pl.ds(column_of, piece)] = jnp.transpose(total).astype(jnp.bfloat16)
     else:
         for s in signs(nz - 1):
@@ -485,10 +486,10 @@
                 pltpu.VMEM((tp, parts, tokens, depth // parts), bf16),
                 pltpu.VMEM((2, rows // PIECES, tp * tokens), bf16),
                 pltpu.VMEM((tp, 2, rows // PIECES, tokens), bf16),
-                pltpu.SemaphoreType.DMA((2 + CUTS + PIECES,)),
+                pltpu.SemaphoreType.DMA((2 + OPENING + PIECES,)),
                 pltpu.SemaphoreType.DMA((4, 2)),
                 pltpu.SemaphoreType.DMA((slots,)),
-                pltpu.SemaphoreType.DMA((3, CUTS)),
+                pltpu.SemaphoreType.DMA((2, CUTS)),
                 pltpu.SemaphoreType.DMA((5,)),
             ],
             compiler_params=pltpu.CompilerParams(

time: 174 us -> 174 us (level)
  no operation moved by 1% of the time
where the time goes in v5:
time: 174 us
  Pallas kernels  173 us (99%)
    pallas_call x1, Pallas kernels, shards(): pl.pallas_call(functools.partial(kernel, nz, ny, tp), out_shape=(pltpu.VM...  167 us
    pallas_call x1, Pallas kernels, shards(): pl.pallas_call(flush, out_shape=(jax.ShapeDtypeStruct((depth, width), bf1...  6.05 us

profile of v5, /device:TPU:0, one launch (start us, length us, event | category | flops | bytes accessed | tf_op | source)
XLA Modules:
  0.0 173.8 jit_solution(1169027969028467269)
XLA Ops:
  0.6 167.2 %shard_map.67 = (bf16[2048,2048]{1,0:T(8,128)(2,1)S(1)}, bf16[2048,2048]{1,0:T(8,128)(2,1)S(1)}, bf16[128,2048]{1,0:T(8,128)(2,1)S(1)}) custom-call(bf16[128,2048]{1,0:T(8,128)(2,1)} %prompt_hbm.1, f32[1,256]{1,0:T(1,128)} %bitcast.1, f32[256,2048]{1,0:T(8,128)} %up_hbm.1, f32[256,2048]{1,0:T(8,128)} %down_hbm.1), custom_call_target="tpu_custom_call" | custom-call | tf_op jit(solution)/shard_map/pallas_call | solution.py:467
  167.8 6.0 %shard_map.68 = (bf16[2048,2048]{1,0:T(8,128)(2,1)}, bf16[2048,2048]{1,0:T(8,128)(2,1)}, bf16[128,2048]{1,0:T(8,128)(2,1)}) custom-call(bf16[2048,2048]{1,0:T(8,128)(2,1)S(1)} %get-tuple-element.6.up_in, bf16[2048,2048]{1,0:T(8,128)(2,1)S(1)} %get-tuple-element.7.down_in, bf16[128,2048]{1,0:T(8,128)(2,1)S(1)} %get-tuple-element.8.mixed_in), custom_call_target="tpu_custom_call" | custom-call | tf_op jit(solution)/shard_map/pallas_call | solution.py:499
